TPU v7x, 32 devices: a whole 2x2x4 slice. The times are simulated.
32 devices in a mesh: ra: 4 (over z), cb: 2 (over y), dp: 4 (over x, core).
Axes of the slice: x: 2, y: 2, z: 4, core: 2. Of those that a mesh axis runs over, the one named last changes fastest.
Arguments:
- tokens: bfloat16 [1792, 4096], P('dp', 'ra'), may hold values from -70 to 70
- norm_in: bfloat16 [4096], P('ra'), may hold values from 0.099609375 to 1.8984375
- w_up: float32 [4096, 16384], P(None, ('ra', 'cb')), may hold values from -0.09375 to 0.09375
- up_scale: float32 [16384], P(('ra', 'cb')), may hold values from 0.5 to 2
- w_down: float32 [16384, 4096], P('ra', 'cb'), may hold values from -0.0625 to 0.0625
- down_scale: float32 [4096], P('cb'), may hold values from 0.5 to 2
- norm_out: float32 [4096], P('cb'), may hold values from 0.1 to 1.9
Outputs:
- result: bfloat16 [1792, 4096], P('dp', 'cb')
All inputs are finite; a program needn't handle non-finite values.
Results may differ from a plain program's by a relative error of at most 0.024.
Values may be sent and summed in bfloat16 or wider, within the bound.
A program may use at most 128 MiB of HBM per device.

v0:
```python
import jax
import jax.numpy as jnp
from jax import lax
from jax.sharding import PartitionSpec as P

epsilon = 1e-06
resid_weight = 0.25


def per_device(tokens, norm_in, w_up, up_scale, w_down, down_scale, norm_out):
    whole_rows, whole_gain = (
        lax.all_gather(tokens, "ra", axis=1, tiled=True),
        lax.all_gather(norm_in, "ra", axis=0, tiled=True),
    )
    whole_float = whole_rows.astype(jnp.float32)
    model_width = whole_float.shape[1]
    inv_in = lax.rsqrt(jnp.mean(whole_float * whole_float, axis=-1) + epsilon)
    normed = (whole_float * whole_gain.astype(jnp.float32)).astype(jnp.bfloat16)
    pre_act = jnp.dot(normed, w_up.astype(jnp.bfloat16), preferred_element_type=jnp.float32)
    pre_act = pre_act * inv_in[:, None] * up_scale
    hidden = jnp.square(jax.nn.relu(pre_act)).astype(jnp.bfloat16)
    down_bf = w_down.astype(jnp.bfloat16)
    quarter = down_bf.shape[1]
    partial_value = jnp.dot(
        lax.all_gather(hidden, "cb", axis=1, tiled=True),
        down_bf,
        preferred_element_type=jnp.float32,
    )
    col_block = lax.axis_index("cb")
    x_quarter = lax.dynamic_slice_in_dim(whole_float, col_block * quarter, quarter, 1)
    down = lax.psum(partial_value.astype(jnp.bfloat16), "ra").astype(jnp.float32)
    mixed = resid_weight * x_quarter + down * down_scale
    total_sq = lax.psum(jnp.sum(mixed * mixed, axis=-1), "cb")
    inv_out = lax.rsqrt(total_sq / model_width + epsilon)
    return (mixed * inv_out[:, None] * norm_out).astype(jnp.bfloat16)


def solution(mesh):
    placed = (
        P("dp", "ra"),
        P("ra"),
        P(None, ("ra", "cb")),
        P(("ra", "cb")),
        P("ra", "cb"),
        P("cb"),
        P("cb"),
    )
    return jax.shard_map(
        per_device, mesh=mesh, in_specs=placed, out_specs=P("dp", "cb"), check_vma=False
    )
```

profile of v0, /device:TPU:0, one launch (start us, length us, event | category | flops | bytes accessed | tf_op | source)
XLA Modules:
  0.0 266.2 jit_solution(17357724036729051572)
XLA Ops:
  6.5 0.0 copy-start.3
  6.5 0.0 all-gather.3.cloned.1.call-start
  6.5 0.7 all-gather.3.cloned.1.call-update
  7.3 0.0 all-gather.5.cloned.1.call-start
  7.3 13.8 %all_gather.10 = bf16[4096]{0:T(1024)(128)(2,1)S(1)} all-gather(bf16[1024]{0:T(1024)(128)(2,1)} %param.8), channel_id=1, replica_groups=mesh['ra'=4,'cb'=2,'dp'=4] {'ra'}, dimensions={0}, use_global_device_ids=true | all-gather | bytes 10240 | tf_op jit(solution)/shard_map/all_gather | solution.py:13
  21.1 62.7 %all-gather.3.cloned.1.call-done = bf16[448,4096]{1,0:T(8,128)(2,1)} async-done(((bf16[448,1024]{1,0:T(8,128)(2,1)}), bf16[448,4096]{1,0:T(8,128)(2,1)}) %all-gather.3.cloned.1.call-update) | async-done | bytes 3670032 | tf_op jit(solution)/shard_map/all_gather | solution.py:12
  83.7 2.8 %multiply_reduce_fusion = f32[448]{0:T(512)S(1)} fusion(bf16[448,4096]{1,0:T(8,128)(2,1)} %all-gather.3.cloned.1.call-done), kind=kLoop, calls=%fused_computation.4 | loop fusion | flops 5504576 | bytes 3671808 | tf_op jit(solution)/shard_map/reduce_sum | solution.py:17
  86.6 0.0 copy-done.3
  86.6 16.5 %multiply_convert_fusion.3 = bf16[448,2048]{1,0:T(8,128)(2,1)} fusion(f32[4096,2048]{1,0:T(8,128)} %param.9, f32[4096]{0:T(1024)S(1)} %convert_element_type.28, bf16[448,4096]{1,0:T(8,128)(2,1)} %all-gather.3.cloned.1.call-done, f32[2048]{0:T(1024)S(1)} %copy-done.3, f32[448]{0:T(512)S(1)} %add_rsqrt_fusion.1), kind=kOutput, calls=%fused_computation.9 | convolution fusion | flops 7534673920 | bytes 39085824 | tf_op jit(solution)/shard_map/dot_general | solution.py:19
  103.1 0.0 all-gather.5.cloned.1.call-update
  103.2 0.0 all-reduce.2.cloned.1.call-start
  103.2 49.5 %all-gather.5.cloned.1.call-done = bf16[448,4096]{1,0:T(8,128)(2,1)} async-done(((bf16[448,2048]{1,0:T(8,128)(2,1)}), bf16[448,4096]{1,0:T(8,128)(2,1)}) %all-gather.5.cloned.1.call-update) | async-done | bytes 3670032 | tf_op jit(solution)/shard_map/all_gather | solution.py:25
  152.7 16.5 %fusion.8 = bf16[448,2048]{1,0:T(8,128)(2,1)} fusion(bf16[448,4096]{1,0:T(8,128)(2,1)} %all-gather.5.cloned.1.call-done, f32[4096,2048]{1,0:T(8,128)} %param.11), kind=kOutput, calls=%fused_computation.12 | convolution fusion | flops 7525498880 | bytes 39059456 | tf_op jit(solution)/shard_map/dot_general | solution.py:24
  169.2 0.0 all-reduce.2.cloned.1.call-update
  169.2 0.0 copy-start.1
  169.2 5.9 %convert_element_type.27 = f32[448,4096]{1,0:T(8,128)} convert(bf16[448,4096]{1,0:T(8,128)(2,1)} %all-gather.3.cloned.1.call-done) | non-fusion elementwise | flops 1835008 | bytes 11010048 | tf_op jit(solution)/shard_map/convert_element_type | solution.py:15
  175.1 0.0 copy-start.2
  175.1 71.8 %all-reduce.2.cloned.1.call-done = bf16[448,2048]{1,0:T(8,128)(2,1)} async-done(((bf16[448,2048]{1,0:T(8,128)(2,1)}), bf16[448,2048]{1,0:T(8,128)(2,1)}) %all-reduce.2.cloned.1.call-update) | async-done | bytes 1835024 | tf_op jit(solution)/shard_map/psum | solution.py:31
  247.0 0.0 copy-done.1
  247.0 0.0 copy-start
  247.0 3.5 %multiply_reduce_fusion.1 = f32[448]{0:T(512)S(1)} fusion(bf16[448,2048]{1,0:T(8,128)(2,1)} %all-reduce.2.cloned.1.call-done, f32[448,4096]{1,0:T(8,128)} %convert_element_type.27, s32[]{:T(128)S(6)} %select_n.3, f32[2048]{0:T(1024)S(1)} %copy-done.1), kind=kLoop, calls=%fused_computation.7 | loop fusion | flops 5504576 | bytes 5515012 | tf_op jit(solution)/shard_map/reduce_sum | solution.py:33
  250.5 4.9 %psum.15 = f32[448]{0:T(512)S(1)} all-reduce(f32[448]{0:T(512)S(1)} %multiply_reduce_fusion.1), channel_id=1, replica_groups=mesh['ra'=4,'cb'=2,'dp'=4] {'cb'}, use_global_device_ids=true, to_apply=%region_3.4 | all-reduce | flops 448 | bytes 3584 | tf_op jit(solution)/shard_map/psum | solution.py:33
  255.4 0.0 copy-done.2
  255.4 0.0 copy-done
  255.4 4.2 %multiply_convert_fusion.2 = bf16[448,2048]{1,0:T(8,128)(2,1)} fusion(bf16[448,2048]{1,0:T(8,128)(2,1)S(1)} %copy-done, f32[448,4096]{1,0:T(8,128)} %convert_element_type.27, s32[]{:T(128)S(6)} %select_n.3, f32[2048]{0:T(1024)S(1)} %copy-done.2, f32[448]{0:T(512)S(1)} %add_rsqrt_fusion, f32[2048]{0:T(1024)S(1)} %copy-done.1), kind=kLoop, calls=%fused_computation.6 | loop fusion | flops 6422528 | bytes 7358212 | tf_op jit(solution)/shard_map/convert_element_type | solution.py:35
  (3 shorter events, 0.0 us)
Async XLA Ops:
  6.5 80.1 %copy-start.3 = (f32[2048]{0:T(1024)S(1)}, f32[2048]{0:T(1024)}, u32[]{:S(2)}) copy-start(f32[2048]{0:T(1024)} %param.10) | copy-start | bytes 24580
  6.5 77.2 %all-gather.3.cloned.1.call-start = ((), (), s32[]{:S(2)}) async-start(), calls=%async_computation | async-start | bytes 4587520 | tf_op jit(solution)/shard_map/all_gather | solution.py:12
  7.3 145.4 %all-gather.5.cloned.1.call-start = ((), (), s32[]{:S(2)}) async-start(), calls=%async_computation.1 | async-start | bytes 5505024 | tf_op jit(solution)/shard_map/all_gather | solution.py:25
  103.2 143.8 %all-reduce.2.cloned.1.call-start = ((), (), s32[]{:S(2)}) async-start(), calls=%async_computation.2 | async-start | bytes 3670016 | tf_op jit(solution)/shard_map/psum | solution.py:31
  169.2 77.8 %copy-start.1 = (f32[2048]{0:T(1024)S(1)}, f32[2048]{0:T(1024)}, u32[]{:S(2)}) copy-start(f32[2048]{0:T(1024)} %param.12) | copy-start | bytes 24580
  175.1 80.3 %copy-start.2 = (f32[2048]{0:T(1024)S(1)}, f32[2048]{0:T(1024)}, u32[]{:S(2)}) copy-start(f32[2048]{0:T(1024)} %param.13) | copy-start | bytes 24580
  247.0 8.5 %copy-start = (bf16[448,2048]{1,0:T(8,128)(2,1)S(1)}, bf16[448,2048]{1,0:T(8,128)(2,1)}, u32[]{:S(2)}) copy-start(bf16[448,2048]{1,0:T(8,128)(2,1)} %all-reduce.2.cloned.1.call-done) | copy-start | bytes 5505028
Sparse Core Ops, SparseCore 0:
  8.9 74.8 all-gather.2
  103.3 49.3 all-gather.4
  169.3 77.5 all-reduce.1
where the time goes:
time: 266 us
  waiting for transfers between devices  185 us (70%)
  matrix products  33 us (12%)
  blocking collectives  18.7 us (7%)
  other arithmetic  16.5 us (6%)
  between operations  13.1 us (5%)
    psum x1, waiting for transfers between devices, per_device(): lax.psum(partial_value.astype(jnp.bfloat16), 'ra').astype(jnp.float32)  71.8 us
    all_gather x1, waiting for transfers between devices, per_device(): lax.all_gather(tokens, 'ra', axis=1, tiled=True)  62.7 us
    all_gather x1, waiting for transfers between devices, per_device(): lax.all_gather(hidden, 'cb', axis=1, tiled=True)  49.5 us
    dot_general x1, matrix products, per_device(): jnp.dot(normed, w_up.astype(jnp.bfloat16), preferred_element_type=jnp.flo...  16.5 us
    dot_general x1, matrix products, per_device(): jnp.dot(lax.all_gather(hidden, 'cb', axis=1, tiled=True), down_bf, prefer...  16.5 us
    all_gather x1, blocking collectives, per_device(): lax.all_gather(norm_in, 'ra', axis=0, tiled=True)  13.8 us
    convert_element_type x1, other arithmetic, per_device(): whole_float = whole_rows.astype(jnp.float32)  5.91 us
  transfers between devices with their start and end apart: 3, of which 3 were waited for; matrix products, arithmetic and copies ran while one was open for 2% of the time, Pallas kernels for 0%

commit v1 on v0

--- a/solution.py
+++ b/solution.py
@@ -1,13 +1,21 @@
+import functools
+
 import jax
 import jax.numpy as jnp
 from jax import lax
+from jax.experimental import pallas as pl
+from jax.experimental.pallas import tpu as pltpu
 from jax.sharding import PartitionSpec as P
 
 epsilon = 1e-06
 resid_weight = 0.25
-
-
-def per_device(tokens, norm_in, w_up, up_scale, w_down, down_scale, norm_out):
+MESH = pl.DeviceIdType.MESH
+CHUNKS = 4
+SLOTS = 6
+STEP_ROWS = 128
+
+
+def plain(tokens, norm_in, w_up, up_scale, w_down, down_scale, norm_out):
     whole_rows, whole_gain = (
         lax.all_gather(tokens, "ra", axis=1, tiled=True),
         lax.all_gather(norm_in, "ra", axis=0, tiled=True),
@@ -35,7 +43,366 @@
     return (mixed * inv_out[:, None] * norm_out).astype(jnp.bfloat16)
 
 
+def kernel(
+    n, chunks,
+    x_ref, gain_ref, wu_ref, us_ref, wd_ref, ds_ref, no_ref,
+    o_ref,
+    xa, gains, wu, wd, stage, normed, hid, parts, rbuf, down, mixed, sq, sqr,
+    load_sem, own_sem, gs, gr,
+    xs, xr, ys, yr, hs, hr, rs, rr, fs, fr, qs, qr,
+):
+    z = lax.axis_index("ra")
+    y = lax.axis_index("cb")
+    twin = 1 - y
+    rows = xa.shape[3]
+    half = xa.shape[4]
+    model_width = 2 * n * half
+    up_cols = wu.shape[1]
+    steps = wu.shape[0] // STEP_ROWS
+
+    def load(ref, i, slot):
+        return pltpu.make_async_copy(
+            ref.at[pl.ds(i * STEP_ROWS, STEP_ROWS)], stage.at[slot], load_sem.at[slot]
+        )
+
+    for i in range(SLOTS):
+        load(wu_ref, i, i).start()
+
+    def own_piece(c, h):
+        return pltpu.make_async_copy(
+            x_ref.at[pl.ds(c * rows, rows), pl.ds(h * half, half)],
+            xa.at[c, z, h],
+            own_sem.at[c, h],
+        )
+
+    for c in range(chunks):
+        for h in range(2):
+            own_piece(c, h).start()
+
+    barrier = pltpu.get_barrier_semaphore()
+    for j in range(1, n):
+        pl.semaphore_signal(
+            barrier, inc=1, device_id={"ra": lax.rem(z + j, n)}, device_id_type=MESH
+        )
+    pl.semaphore_signal(barrier, inc=1, device_id={"cb": twin}, device_id_type=MESH)
+    pl.semaphore_wait(barrier, n)
+
+    def remote(src, dst, send, recv, where):
+        return pltpu.make_async_remote_copy(
+            src_ref=src, dst_ref=dst, send_sem=send, recv_sem=recv,
+            device_id=where, device_id_type=MESH,
+        )
+
+    def x_copy(c, src, way):
+        piece = xa.at[c, src, y]
+        return remote(piece, piece, xs.at[c, src, way], xr.at[c, src], {"ra": z + 1 - 2 * way})
+
+    def y_copy(c, src):
+        piece = xa.at[c, src, y]
+        return remote(piece, piece, ys.at[c, src], yr.at[c, src], {"cb": twin})
+
+    def y_arrive(c, src):
+        piece = xa.at[c, src, twin]
+        return remote(piece, piece, ys.at[c, src], yr.at[c, src], {"cb": twin})
+
+    def d_copy(c, src, way):
+        piece = down.at[c, src]
+        return remote(piece, piece, fs.at[c, src, way], fr.at[c, src], {"ra": z + 1 - 2 * way})
+
+    def start_line(copy, c):
+        @pl.when(z + 1 < n)
+        def _():
+            copy(c, z, 0).start()
+
+        @pl.when(z > 0)
+        def _():
+            copy(c, z, 1).start()
+
+    def relay(copy, c, k, also=None):
+        @pl.when(z - k >= 0)
+        def _():
+            src = z - k
+            copy(c, src, 0).wait_recv()
+
+            @pl.when(z + 1 < n)
+            def _():
+                copy(c, src, 0).start()
+
+            if also is not None:
+                also(c, src).start()
+
+        @pl.when(z + k < n)
+        def _():
+            src = z + k
+            copy(c, src, 1).wait_recv()
+
+            @pl.when(z > 0)
+            def _():
+                copy(c, src, 1).start()
+
+            if also is not None:
+                also(c, src).start()
+
+    def gain_copy(where, src):
+        return remote(gain_ref, gains.at[src], gs.at[where], gr.at[src], {"ra": where})
+
+    def begin(c):
+        if c < chunks:
+            for h in range(2):
+                own_piece(c, h).wait()
+            start_line(x_copy, c)
+
+    begin(0)
+    for j in range(1, n):
+        gain_copy(lax.rem(z + j, n), z).start()
+    gains[z] = gain_ref[...]
+    begin(1)
+
+    def gather_step(c, k):
+        relay(x_copy, c, k, y_copy)
+        if k == 1:
+            begin(c + 2)
+
+    def convert(ref, target, following, lo, hi):
+        def body(i, carry):
+            slot = lax.rem(i + (0 if following is not None else steps), SLOTS)
+            load(ref, i, slot).wait()
+            target[pl.ds(pl.multiple_of(i * STEP_ROWS, STEP_ROWS), STEP_ROWS), :] = stage[
+                slot
+            ].astype(jnp.bfloat16)
+
+            @pl.when(i + SLOTS < steps)
+            def _():
+                load(ref, i + SLOTS, slot).start()
+
+            if following is not None:
+                @pl.when(i + SLOTS >= steps)
+                def _():
+                    load(following, i + SLOTS - steps, slot).start()
+
+            return carry
+
+        lax.fori_loop(lo, hi, body, 0)
+
+    def convert_with_gather(ref, target, following, c):
+        cuts = [steps * k // n for k in range(n + 1)]
+        for k in range(1, n + 1):
+            convert(ref, target, following, cuts[k - 1], cuts[k])
+            if k < n and c < chunks:
+                gather_step(c, k)
+
+    def hid_copy(c, block):
+        piece = hid.at[c, block]
+        return remote(piece, piece, hs.at[c], hr.at[c], {"cb": twin})
+
+    def up(c):
+        for j in range(1, n):
+            y_arrive(c, lax.rem(z + j, n)).wait_recv()
+        total = jnp.zeros((rows, 1), jnp.float32)
+        for s in range(n):
+            for h in range(2):
+                xf = xa[c, s, h].astype(jnp.float32)
+                total += jnp.sum(xf * xf, axis=1, keepdims=True)
+                gain = gains[s][:, h * half : (h + 1) * half]
+                lo = (2 * s + h) * half
+                normed[:, lo : lo + half] = (xf * gain).astype(jnp.bfloat16)
+        inv_in = lax.rsqrt(total / model_width + epsilon)
+        tile = 256
+
+        def body(j, carry):
+            cols = pl.ds(pl.multiple_of(j * tile, tile), tile)
+            pre = jnp.dot(normed[...], wu[:, cols], preferred_element_type=jnp.float32)
+            pre = jnp.maximum(pre * inv_in * us_ref[:, cols], 0.0)
+            hid[c, y, :, cols] = (pre * pre).astype(jnp.bfloat16)
+            return carry
+
+        lax.fori_loop(0, up_cols // tile, body, 0)
+        hid_copy(c, y).start()
+
+    def part_copy(c, where, src):
+        return remote(
+            parts.at[c, where], rbuf.at[c, src], rs.at[c, where], rr.at[c, src], {"ra": where}
+        )
+
+    def down_product(c):
+        hid_copy(c, twin).wait_recv()
+
+        def body(q, carry):
+            cols = pl.ds(pl.multiple_of(q * half, half), half)
+            acc = jnp.dot(hid[c, 0], wd[:up_cols, cols], preferred_element_type=jnp.float32)
+            acc += jnp.dot(hid[c, 1], wd[up_cols:, cols], preferred_element_type=jnp.float32)
+            parts[c, q] = acc.astype(jnp.bfloat16)
+            return carry
+
+        lax.fori_loop(0, n, body, 0)
+        for j in range(1, n):
+            part_copy(c, lax.rem(z + j, n), z).start()
+
+    def reduce(c):
+        acc = parts[c, z].astype(jnp.float32)
+        for j in range(1, n):
+            src = lax.rem(z + j, n)
+            part_copy(c, src, src).wait_recv()
+            acc += rbuf[c, src].astype(jnp.float32)
+        down[c, z] = acc.astype(jnp.bfloat16)
+        start_line(d_copy, c)
+
+    def sq_copy(c):
+        return remote(sq.at[c], sqr.at[c], qs.at[c], qr.at[c], {"cb": twin})
+
+    def mix(c):
+        for k in range(1, n):
+            relay(d_copy, c, k)
+        total = jnp.zeros((rows, 1), jnp.float32)
+        for q in range(n):
+            cols = slice(q * half, (q + 1) * half)
+            at = y * n + q
+            resid = xa[c, at // 2, at % 2].astype(jnp.float32)
+            value = resid_weight * resid + down[c, q].astype(jnp.float32) * ds_ref[:, cols]
+            mixed[c % 2, :, cols] = value
+            total += jnp.sum(value * value, axis=1, keepdims=True)
+        sq[c] = jnp.broadcast_to(total, (rows, 128))
+        sq_copy(c).start()
+
+    def finish(c):
+        sq_copy(c).wait_recv()
+        total = sq[c][:, :1] + sqr[c][:, :1]
+        inv_out = lax.rsqrt(total / model_width + epsilon)
+        o_ref[c * rows : (c + 1) * rows, :] = (mixed[c % 2] * inv_out * no_ref[...]).astype(
+            jnp.bfloat16
+        )
+
+    convert_with_gather(wu_ref, wu, wd_ref, 0)
+    for j in range(1, n):
+        src = lax.rem(z + j, n)
+        gain_copy(src, src).wait_recv()
+    up(0)
+    convert_with_gather(wd_ref, wd, None, 1)
+    for t in range(1, chunks + 4):
+        if t < chunks:
+            if t > 1:
+                for k in range(1, n):
+                    gather_step(t, k)
+            up(t)
+        if 0 <= t - 1 < chunks:
+            down_product(t - 1)
+        if 0 <= t - 2 < chunks:
+            reduce(t - 2)
+        if 0 <= t - 4 < chunks:
+            finish(t - 4)
+        if 0 <= t - 3 < chunks:
+            mix(t - 3)
+
+    for j in range(1, n):
+        gain_copy(lax.rem(z + j, n), z).wait_send()
+
+    def drain(c, carry):
+        for src in range(n):
+            @pl.when((src <= z) & (z + 1 < n))
+            def _():
+                x_copy(c, src, 0).wait_send()
+                d_copy(c, src, 0).wait_send()
+
+            @pl.when((src >= z) & (z > 0))
+            def _():
+                x_copy(c, src, 1).wait_send()
+                d_copy(c, src, 1).wait_send()
+
+            @pl.when(z != src)
+            def _():
+                y_copy(c, src).wait_send()
+                part_copy(c, src, z).wait_send()
+
+        hid_copy(c, y).wait_send()
+        sq_copy(c).wait_send()
+        return carry
+
+    lax.fori_loop(0, chunks, drain, 0)
+
+
+def fused(n, tokens, norm_in, w_up, up_scale, w_down, down_scale, norm_out):
+    chunks = CHUNKS
+    rows = tokens.shape[0] // chunks
+    half = tokens.shape[1] // 2
+    wide = w_down.shape[1]
+    bf16, f32 = jnp.bfloat16, jnp.float32
+    dma = pltpu.SemaphoreType.DMA
+    vmem = pl.BlockSpec(memory_space=pltpu.VMEM)
+    far = pl.BlockSpec(memory_space=pl.ANY)
+    flops = 2 * tokens.shape[0] * (w_up.size + w_down.size)
+    return pl.pallas_call(
+        functools.partial(kernel, n, chunks),
+        out_shape=jax.ShapeDtypeStruct((tokens.shape[0], wide), bf16),
+        in_specs=[far, vmem, far, vmem, far, vmem, vmem],
+        out_specs=vmem,
+        scratch_shapes=[
+            pltpu.VMEM((chunks, n, 2, rows, half), bf16),
+            pltpu.VMEM((n, 1, 2 * half), f32),
+            pltpu.VMEM(w_up.shape, bf16),
+            pltpu.VMEM(w_down.shape, bf16),
+            pltpu.VMEM((SLOTS, STEP_ROWS, wide), f32),
+            pltpu.VMEM((rows, 2 * half * n), bf16),
+            pltpu.VMEM((chunks, 2, rows, w_up.shape[1]), bf16),
+            pltpu.VMEM((chunks, n, rows, half), bf16),
+            pltpu.VMEM((chunks, n, rows, half), bf16),
+            pltpu.VMEM((chunks, n, rows, half), bf16),
+            pltpu.VMEM((2, rows, wide), f32),
+            pltpu.VMEM((chunks, rows, 128), f32),
+            pltpu.VMEM((chunks, rows, 128), f32),
+            dma((SLOTS,)),
+            dma((chunks, 2)),
+            dma((n,)),
+            dma((n,)),
+            dma((chunks, n, 2)),
+            dma((chunks, n)),
+            dma((chunks, n)),
+            dma((chunks, n)),
+            dma((chunks,)),
+            dma((chunks,)),
+            dma((chunks, n)),
+            dma((chunks, n)),
+            dma((chunks, n, 2)),
+            dma((chunks, n)),
+            dma((chunks,)),
+            dma((chunks,)),
+        ],
+        compiler_params=pltpu.CompilerParams(
+            collective_id=0, has_side_effects=True, vmem_limit_bytes=67043328
+        ),
+        cost_estimate=pl.CostEstimate(
+            flops=flops, bytes_accessed=4 * (w_up.size + w_down.size), transcendentals=0
+        ),
+    )(
+        tokens,
+        norm_in.astype(f32)[None, :],
+        w_up,
+        up_scale[None, :],
+        w_down,
+        down_scale[None, :],
+        norm_out[None, :],
+    )
+
+
 def solution(mesh):
+    n, m = mesh.shape["ra"], mesh.shape["cb"]
+
+    def per_device(tokens, norm_in, w_up, up_scale, w_down, down_scale, norm_out):
+        args = (tokens, norm_in, w_up, up_scale, w_down, down_scale, norm_out)
+        fits = (
+            m == 2
+            and n > 1
+            and CHUNKS > 1
+            and tokens.shape[0] % (CHUNKS * 16) == 0
+            and tokens.shape[1] % 256 == 0
+            and w_up.shape == w_down.shape
+            and w_up.shape[0] % (STEP_ROWS * n) == 0
+            and w_up.shape[0] // STEP_ROWS >= SLOTS
+            and w_up.shape[1] % 256 == 0
+            and w_up.size <= 8 * 1024 * 1024
+            and tokens.size * n <= 2 * 1024 * 1024
+        )
+        return fused(n, *args) if fits else plain(*args)
+
     placed = (
         P("dp", "ra"),
         P("ra"),

time: 266 us -> 157 us (0.59)
  waiting for transfers between devices: 185 us -> 0 us
  Pallas kernels: 0 us -> 153 us
  matrix products: 33 us -> 0 us
  blocking collectives: 18.7 us -> 0 us
  other arithmetic: 16.5 us -> 1.27 us
  between operations: 13.1 us -> 0.01 us
  local copies, waits for them, and re-layouts: 0.02 us -> 2.94 us
    pallas_call x0 -> x1, Pallas kernels: none -> 153 us  [fused(): pl.pallas_call(functools.partial(kernel, n, chunks), out_shape=jax.ShapeD...]
    all_gather x2 -> x0, waiting for transfers between devices: 112 us -> none  [the longest x1 62.7 us: per_device(): lax.all_gather(tokens, 'ra', axis=1, tiled=True)]
    psum x1 -> x0, waiting for transfers between devices: 71.8 us -> none  [per_device(): lax.psum(partial_value.astype(jnp.bfloat16), 'ra').astype(jnp.float32)]
    dot_general x2 -> x0, matrix products: 33 us -> none  [the longest x1 16.5 us: per_device(): jnp.dot(normed, w_up.astype(jnp.bfloat16), preferred_element_type=jnp.flo...]
    all_gather x1 -> x0, blocking collectives: 13.8 us -> none  [per_device(): lax.all_gather(norm_in, 'ra', axis=0, tiled=True)]
    convert_element_type x3 -> x0, other arithmetic: 10.2 us -> none  [the longest x1 5.91 us: per_device(): whole_float = whole_rows.astype(jnp.float32)]
    reduce_sum x2 -> x0, other arithmetic: 6.34 us -> none  [the longest x1 3.51 us: per_device(): total_sq = lax.psum(jnp.sum(mixed * mixed, axis=-1), 'cb')]
    psum x1 -> x0, blocking collectives: 4.93 us -> none  [per_device(): total_sq = lax.psum(jnp.sum(mixed * mixed, axis=-1), 'cb')]
  transfers between devices with their start and end apart: 3 -> 0, of which waited for: 3 -> 0; matrix products, arithmetic and copies ran while one was open for 2% -> 0% of each run, Pallas kernels for 0% -> 0%
where the time goes in v1:
time: 157 us
  Pallas kernels  153 us (97%)
  local copies, waits for them, and re-layouts  2.94 us (2%)
    pallas_call x1, Pallas kernels, fused(): pl.pallas_call(functools.partial(kernel, n, chunks), out_shape=jax.ShapeD...  153 us

profile of v1, /device:TPU:0, one launch (start us, length us, event | category | flops | bytes accessed | tf_op | source)
XLA Modules:
  0.0 157.2 jit_solution(5524423995310465143)
XLA Ops:
  0.0 1.3 broadcast_in_dim.19
  1.3 153.0 %shard_map.73 = bf16[448,2048]{1,0:T(8,128)(2,1)} custom-call(bf16[448,1024]{1,0:T(8,128)(2,1)} %x_ref.1, f32[1,1024]{1,0:T(1,128)} %bitcast.4, f32[4096,2048]{1,0:T(8,128)} %wu_ref.1, f32[1,2048]{1,0:T(1,128)} %bitcast.5, f32[4096,2048]{1,0:T(8,128)} %wd_ref.1, f32[1,2048]{1,0:T(1,128)} %bitcast.6, f32[1,2048]{1,0:T(1,128)} %bitcast.7), custom_call_target="tpu_custom_call" | custom-call | flops 15032385536 | bytes 67108864 | tf_op jit(solution)/shard_map/pallas_call | solution.py:333
  154.2 2.9 %copy.9 = bf16[448,2048]{1,0:T(8,128)(2,1)} copy(bf16[448,2048]{1,0:T(8,128)(2,1)} %shard_map.73) | data formatting | bytes 3670016

commit v2 on v1

--- a/solution.py
+++ b/solution.py
@@ -184,12 +184,13 @@
 
         lax.fori_loop(lo, hi, body, 0)
 
-    def convert_with_gather(ref, target, following, c):
-        cuts = [steps * k // n for k in range(n + 1)]
-        for k in range(1, n + 1):
-            convert(ref, target, following, cuts[k - 1], cuts[k])
-            if k < n and c < chunks:
-                gather_step(c, k)
+    def convert_with_gather(ref, target, following, among):
+        relays = [(c, k) for c in among if c < chunks for k in range(1, n)]
+        cuts = [steps * k // (len(relays) + 1) for k in range(len(relays) + 2)]
+        for i in range(len(relays) + 1):
+            convert(ref, target, following, cuts[i], cuts[i + 1])
+            if i < len(relays):
+                gather_step(*relays[i])
 
     def hid_copy(c, block):
         piece = hid.at[c, block]
@@ -251,8 +252,6 @@
         return remote(sq.at[c], sqr.at[c], qs.at[c], qr.at[c], {"cb": twin})
 
     def mix(c):
-        for k in range(1, n):
-            relay(d_copy, c, k)
         total = jnp.zeros((rows, 1), jnp.float32)
         for q in range(n):
             cols = slice(q * half, (q + 1) * half)
@@ -272,20 +271,27 @@
             jnp.bfloat16
         )
 
-    convert_with_gather(wu_ref, wu, wd_ref, 0)
+    convert_with_gather(wu_ref, wu, wd_ref, (0,))
     for j in range(1, n):
         src = lax.rem(z + j, n)
         gain_copy(src, src).wait_recv()
     up(0)
-    convert_with_gather(wd_ref, wd, None, 1)
+    convert_with_gather(wd_ref, wd, None, (1, 2))
+    def spread(c, lo, hi):
+        if 0 <= c < chunks:
+            for k in range(lo, hi):
+                relay(d_copy, c, k)
+
     for t in range(1, chunks + 4):
         if t < chunks:
-            if t > 1:
-                for k in range(1, n):
-                    gather_step(t, k)
             up(t)
+        spread(t - 3, 1, 2)
         if 0 <= t - 1 < chunks:
             down_product(t - 1)
+        spread(t - 3, 2, n)
+        if 2 < t + 2 < chunks:
+            for k in range(1, n):
+                gather_step(t + 2, k)
         if 0 <= t - 2 < chunks:
             reduce(t - 2)
         if 0 <= t - 4 < chunks:

time: 157 us -> 145 us (0.924)
  Pallas kernels: 153 us -> 140 us
    pallas_call x1, Pallas kernels: 153 us -> 140 us  [fused(): pl.pallas_call(functools.partial(kernel, n, chunks), out_shape=jax.ShapeD...]
where the time goes in v2:
time: 145 us
  Pallas kernels  140 us (97%)
  local copies, waits for them, and re-layouts  2.94 us (2%)
    pallas_call x1, Pallas kernels, fused(): pl.pallas_call(functools.partial(kernel, n, chunks), out_shape=jax.ShapeD...  140 us
    unnamed x1, local copies, waits for them, and re-layouts  2.94 us

profile of v2, /device:TPU:0, one launch (start us, length us, event | category | flops | bytes accessed | tf_op | source)
XLA Modules:
  0.0 144.5 jit_solution(18226311986950524008)
XLA Ops:
  0.0 1.3 broadcast_in_dim.19
  1.3 140.3 %shard_map.73 = bf16[448,2048]{1,0:T(8,128)(2,1)} custom-call(bf16[448,1024]{1,0:T(8,128)(2,1)} %x_ref.1, f32[1,1024]{1,0:T(1,128)} %bitcast.4, f32[4096,2048]{1,0:T(8,128)} %wu_ref.1, f32[1,2048]{1,0:T(1,128)} %bitcast.5, f32[4096,2048]{1,0:T(8,128)} %wd_ref.1, f32[1,2048]{1,0:T(1,128)} %bitcast.6, f32[1,2048]{1,0:T(1,128)} %bitcast.7), custom_call_target="tpu_custom_call" | custom-call | flops 15032385536 | bytes 67108864 | tf_op jit(solution)/shard_map/pallas_call | solution.py:339
  141.6 2.9 %copy.9 = bf16[448,2048]{1,0:T(8,128)(2,1)} copy(bf16[448,2048]{1,0:T(8,128)(2,1)} %shard_map.73) | data formatting | bytes 3670016
